TPU v7x, 512 devices: a whole 4x8x8 slice. The times are simulated.
512 devices in a mesh: sp: 64 (over z, y), tp: 4 (over x), dp: 2 (over core).
Axes of the slice: x: 4, y: 8, z: 8, core: 2. Of those that a mesh axis runs over, the one named last changes fastest.
Arguments:
- latent: bfloat16 [2, 16384, 2048], P('dp', ('sp', 'tp')), may hold values from -6 to 6
- condition: bfloat16 [2, 2048], P('dp', ('sp', 'tp')), may hold values from -6 to 6
- context: bfloat16 [2, 512, 2048], P('dp', 'sp'), may hold values from -6 to 6
- context_vector: bfloat16 [2048], P(('sp', 'tp')), may hold values from -6 to 6
- modulator: bfloat16 [2048, 6144], P(('sp', 'tp')), may hold values from -0.3125 to 0.3125
- norm_gain: float32 [2048], replicated, may hold values from 0.1 to 1.9
- query_weight: bfloat16 [2048, 512], P(None, 'tp'), may hold values from -4 to 4
- key_weight: bfloat16 [2048, 512], P(None, 'tp'), may hold values from -0.125 to 0.125
- value_weight: bfloat16 [2048, 512], P(None, 'tp'), may hold values from -0.125 to 0.125
- head_gain: float32 [128], replicated, may hold values from 0.1 to 1.9
- lambdas: float32 [4], P('tp'), may hold values from 0.3 to 0.8
- context_bias: float32 [4, 2], P('tp'), may hold values from 1.3 to 2.7
- out_weight: bfloat16 [512, 2048], P('tp'), may hold values from -0.25 to 0.25
Outputs:
- updated: bfloat16 [2, 16384, 2048], P('dp', ('sp', 'tp'))
All inputs are finite; a program needn't handle non-finite values.
Results may differ from a plain program's by a relative error of at most 0.024.
Values may be sent and summed in bfloat16 or wider, within the bound.
A program may use at most 64 MiB of HBM per device.

v0:
```python
import jax
import jax.numpy as jnp
from jax import lax
from jax.sharding import Mesh
from jax.sharding import PartitionSpec as P

SP_TP = ("sp_0", "sp_1", "tp")
SP = ("sp_0", "sp_1")
EPSILON = 1e-06
OUT_SCALE = 0.8
KEY_BLOCK = 2048
LOW_START = -1e30


def by_axis(shard, axes):
    for axis in axes:
        shard = lax.psum(shard, axis)
    return shard


def joined_along(blocks, dim):
    lengths = list(blocks.shape[1:])
    lengths[dim] *= blocks.shape[0]
    return jnp.moveaxis(blocks, 0, dim).reshape(lengths)


def sent_to_all(shard, axis):
    copies = jnp.broadcast_to(shard, (lax.axis_size(axis), *shard.shape))
    return lax.all_to_all(copies, axis, split_axis=0, concat_axis=0, tiled=True)


def gather_directly(shard, axis, dim):
    return joined_along(sent_to_all(shard, axis), dim)


def sent_together(arrays, axis, dim, along):
    ends, at = ([], 0)
    for a in arrays[:-1]:
        at += a.shape[along]
        ends.append(at)
    both = jnp.concatenate(arrays, axis=along)
    return tuple(jnp.split(lax.all_gather(both, axis, axis=dim, tiled=True), ends, axis=along))


def split_up(shard, dim, devices):
    lengths = shard.shape
    blocks = shard.reshape(*lengths[:dim], devices, lengths[dim] // devices, *lengths[dim + 1 :])
    return jnp.moveaxis(blocks, dim, 0)


def summed_on_arrival(shard, axis, dim):
    blocks = split_up(shard, dim, lax.axis_size(axis))
    arrived = lax.all_to_all(blocks, axis, split_axis=0, concat_axis=0, tiled=True)
    return arrived.astype(jnp.float32).sum(axis=0)


def modulate(inputs, gain_vector, shift_vector, scale_vector):
    as_float = inputs.astype(jnp.float32)
    normed = as_float * lax.rsqrt(jnp.mean(as_float * as_float, axis=-1, keepdims=True) + EPSILON)
    return (normed * gain_vector * (1.0 + scale_vector) + shift_vector).astype(jnp.bfloat16)


def fold_block(running, queries, keys_in, values_in, key_flags, bias_table, score_scale):
    run_max, run_total, summed = running
    scores = (
        jnp.einsum("qhmd,khmd->hmqk", queries, keys_in, preferred_element_type=jnp.float32)
        * score_scale
    )
    if key_flags is not None:
        scores = scores + bias_table[:, :, None, None] * key_flags
    new_max = jnp.maximum(run_max, jnp.max(scores, axis=-1))
    shrink = jnp.exp(run_max - new_max)
    weights = jnp.exp(scores - new_max[..., None])
    run_total = run_total * shrink + jnp.sum(weights, axis=-1)
    summed = summed * shrink[..., None] + jnp.einsum(
        "hmqk,khe->hmqe",
        weights.astype(jnp.bfloat16),
        values_in,
        preferred_element_type=jnp.float32,
    )
    return (new_max, run_total, summed)


def fold_keys(running, queries, keys_in, values_in, key_flags, bias_table, score_scale):
    full_blocks = keys_in.shape[0] // KEY_BLOCK
    if full_blocks > 1:
        edge = full_blocks * KEY_BLOCK
        stacked = (
            keys_in.reshape((full_blocks, KEY_BLOCK) + keys_in.shape[1:]),
            values_in.reshape((full_blocks, KEY_BLOCK) + values_in.shape[1:]),
        )

        def fold_step(current, block_data):
            flag_part = None
            return (
                fold_block(
                    current,
                    queries,
                    block_data[0],
                    block_data[1],
                    flag_part,
                    bias_table,
                    score_scale,
                ),
                None,
            )

        running, ignored = lax.scan(fold_step, running, stacked)
        keys_in = keys_in[edge:]
        values_in = values_in[edge:]
        key_flags = None
    if keys_in.shape[0] > 0:
        running = fold_block(
            running, queries, keys_in, values_in, key_flags, bias_table, score_scale
        )
    return running


def body(
    latent,
    condition,
    context,
    context_vector,
    modulator,
    norm_gain,
    query_weight,
    key_weight,
    value_weight,
    head_gain,
    lambdas,
    context_bias,
    out_weight,
):
    model_width = latent.shape[2]
    local_heads = lambdas.shape[0]
    query_width = query_weight.shape[1]
    head_size = query_width // (2 * local_heads)
    value_size = value_weight.shape[1] // local_heads
    score_scale = head_size ** (-0.5)
    activated = jax.nn.silu(
        jnp.concatenate([condition, context_vector[None, :]], axis=0).astype(jnp.float32)
    )
    partial_terms = jnp.dot(
        activated.astype(jnp.bfloat16), modulator, preferred_element_type=jnp.float32
    )
    modulations = by_axis(partial_terms, SP_TP)
    hidden = modulate(
        latent[0],
        norm_gain,
        modulations[0, :model_width],
        modulations[0, model_width : 2 * model_width],
    )
    ctx_hidden = modulate(
        context[0],
        norm_gain,
        modulations[1, :model_width],
        modulations[1, model_width : 2 * model_width],
    )
    gate_vector = modulations[0, 2 * model_width :]
    incoming = gather_directly(hidden, "tp", 0)
    projected = jnp.concatenate(
        [
            jnp.dot(incoming, query_weight, preferred_element_type=jnp.float32),
            jnp.dot(incoming, key_weight, preferred_element_type=jnp.float32),
            jnp.dot(incoming, value_weight, preferred_element_type=jnp.float32),
        ],
        axis=1,
    ).astype(jnp.bfloat16)
    query_rows = projected.shape[0]
    queries = projected[:, :query_width].reshape(query_rows, local_heads, 2, head_size)
    own_keys = projected[:, query_width : 2 * query_width]
    own_values = projected[:, 2 * query_width :]
    ctx_keys = jnp.dot(ctx_hidden, key_weight, preferred_element_type=jnp.float32).astype(
        jnp.bfloat16
    )
    ctx_values = jnp.dot(ctx_hidden, value_weight, preferred_element_type=jnp.float32).astype(
        jnp.bfloat16
    )
    ctx_keys, ctx_values = sent_together((ctx_keys, ctx_values), SP, 0, 1)
    start_carry = (
        jnp.full((local_heads, 2, query_rows), LOW_START, jnp.float32),
        jnp.zeros((local_heads, 2, query_rows), jnp.float32),
        jnp.zeros((local_heads, 2, query_rows, value_size), jnp.float32),
    )
    pieces = (own_keys, own_values)
    initial = fold_keys(
        start_carry,
        queries,
        ctx_keys.reshape(-1, local_heads, 2, head_size),
        ctx_values.reshape(-1, local_heads, value_size),
        jnp.ones((ctx_keys.shape[0],), jnp.float32),
        context_bias,
        score_scale,
    )
    incoming = sent_together((pieces[0], pieces[1]), SP, 0, 1)
    run_max, run_total, summed = fold_keys(
        initial,
        queries,
        incoming[0].reshape(-1, local_heads, 2, head_size),
        incoming[1].reshape(-1, local_heads, value_size),
        None,
        context_bias,
        score_scale,
    )
    mixed = (
        summed[:, 0] / run_total[:, 0, :, None]
        - lambdas[:, None, None] * summed[:, 1] / run_total[:, 1, :, None]
    )
    normed = (
        mixed
        * lax.rsqrt(jnp.mean(mixed * mixed, axis=-1, keepdims=True) + EPSILON)
        * head_gain
        * OUT_SCALE
    )
    attended = (
        jnp.transpose(normed, (1, 0, 2))
        .reshape(query_rows, local_heads * value_size)
        .astype(jnp.bfloat16)
    )
    branch = summed_on_arrival(
        jnp.dot(attended, out_weight, preferred_element_type=jnp.float32).astype(jnp.bfloat16),
        "tp",
        0,
    )
    result = (latent[0].astype(jnp.float32) + gate_vector * branch).astype(jnp.bfloat16)
    return result[None]


def solution(mesh):
    torus = Mesh(
        mesh.devices.reshape(8, 8, mesh.shape["tp"], mesh.shape["dp"]), ("sp_0", "sp_1", "tp", "dp")
    )
    return jax.shard_map(
        body,
        mesh=torus,
        in_specs=(
            P("dp", SP_TP, None),
            P("dp", SP_TP),
            P("dp", SP, None),
            P(SP_TP),
            P(SP_TP, None),
            P(),
            P(None, "tp"),
            P(None, "tp"),
            P(None, "tp"),
            P(),
            P("tp"),
            P("tp", None),
            P("tp", None),
        ),
        out_specs=P("dp", SP_TP, None),
        check_vma=False,
    )
```

profile of v0, /device:TPU:8, one launch (start us, length us, event | category | flops | bytes accessed | tf_op | source)
XLA Modules:
  0.0 289.6 jit_solution(1332967432429290090)
XLA Ops:
  6.6 1.2 fusion.60
  7.8 36.4 %psum.21 = f32[2,6144]{1,0:T(2,128)S(1)} all-reduce(f32[2,6144]{1,0:T(2,128)S(1)} %fusion.60), channel_id=1, replica_groups=mesh['sp_0'=8,'sp_1'=8,'tp'=4,'dp'=2] {'sp_0'}, use_global_device_ids=true, to_apply=%region_0.1 | all-reduce | flops 12288 | bytes 98304 | tf_op jit(solution)/shard_map/psum | solution.py:17
  44.2 28.8 %psum.22 = f32[2,6144]{1,0:T(2,128)S(1)} all-reduce(f32[2,6144]{1,0:T(2,128)S(1)} %psum.21), channel_id=1, replica_groups=mesh['sp_0'=8,'sp_1'=8,'tp'=4,'dp'=2] {'sp_1'}, use_global_device_ids=true, to_apply=%region_1.2 | all-reduce | flops 12288 | bytes 98304 | tf_op jit(solution)/shard_map/psum | solution.py:17
  72.9 17.9 %psum.23 = f32[2,6144]{1,0:T(2,128)S(1)} all-reduce(f32[2,6144]{1,0:T(2,128)S(1)} %psum.22), channel_id=1, replica_groups=mesh['sp_0'=8,'sp_1'=8,'tp'=4,'dp'=2] {'tp'}, use_global_device_ids=true, to_apply=%region_2.3 | all-reduce | flops 12288 | bytes 98304 | tf_op jit(solution)/shard_map/psum | solution.py:17
  90.9 1.1 fusion.29
  92.0 1.1 fusion.33
  93.3 13.5 %all_to_all.10 = bf16[4,64,2048]{2,1,0:T(8,128)(2,1)S(1)} all-to-all(bf16[4,64,2048]{2,1,0:T(8,128)(2,1)S(1)} %broadcast_in_dim.13), channel_id=1, replica_groups=mesh['sp_0'=8,'sp_1'=8,'tp'=4,'dp'=2] {'tp'}, dimensions={0} | all-to-all | bytes 2097152 | tf_op jit(solution)/shard_map/all_to_all | solution.py:29
  106.8 0.5 convolution_convert_fusion.1
  107.3 0.5 convolution_convert_fusion.2
  107.8 0.7 pad_maximum_fusion
  109.1 49.1 %all_gather.6 = bf16[512,256]{1,0:T(8,128)(2,1)S(1)} all-gather(bf16[8,256]{1,0:T(8,128)(2,1)S(1)} %pad_maximum_fusion.1), channel_id=1, replica_groups=mesh['sp_0'=8,'sp_1'=8,'tp'=4,'dp'=2] {'sp_0','sp_1'}, dimensions={0}, use_global_device_ids=true | all-gather | bytes 266240 | tf_op jit(solution)/shard_map/all_gather | solution.py:42
  159.0 0.5 convolution_convert_fusion.3
  159.5 0.4 fusion.75
  160.0 0.3 fusion.26
  160.3 0.4 fusion.24
  160.7 50.3 %all-gather.2.cloned.1.call-done = bf16[16384,256]{0,1:T(8,128)(2,1)} async-done(((bf16[256,256]{0,1:T(8,128)(2,1)}), bf16[16384,256]{0,1:T(8,128)(2,1)}) %all-gather.2.cloned.1.call-update) | async-done | bytes 8388624 | tf_op jit(solution)/shard_map/all_gather | solution.py:42
  211.0 5.0 %fusion.72 = (bf16[16384,128]{0,1:T(8,128)(2,1)}, bf16[16384,128]{0,1:T(8,128)(2,1)S(1)}) fusion(bf16[16384,256]{0,1:T(8,128)(2,1)} %all-gather.2.cloned.1.call-done), kind=kLoop, calls=%fused_computation.100 | loop fusion | bytes 16777216 | tf_op jit(solution)/shard_map/split | solution.py:42
  216.0 3.2 %copy.24 = bf16[16,8,8,2048]{3,2,1,0:T(8,128)(2,1)S(1)} copy(bf16[16,8,8,2048]{3,1,2,0:T(8,128)(2,1)S(1)} %bitcast.170) | data formatting | bytes 8388608
  219.2 4.2 %copy.20 = bf16[8,2048,1,2,64]{1,4,3,2,0:T(8,128)(2,1)} copy(bf16[8,2048,1,2,64]{1,0,4,3,2:T(8,128)(2,1)S(1)} %bitcast.166) | data formatting | bytes 8388608 | tf_op jit(solution)/shard_map/while | solution.py:108
  223.4 6.4 %copy.23 = bf16[16384,128]{1,0:T(8,128)(2,1)} copy(bf16[16384,128]{0,1:T(8,128)(2,1)} %get-tuple-element.77) | data formatting | bytes 8388608 | tf_op jit(solution)/shard_map/while | solution.py:108
  229.8 36.3 %while.14 = (s32[]{:T(128)}, f32[1,2,256]{2,1,0:T(2,128)S(1)}, f32[1,2,256]{2,1,0:T(2,128)S(1)}, f32[1,2,256,128]{3,2,1,0:T(8,128)S(1)}, bf16[8,2048,1,2,64]{1,4...) while((s32[]{:T(128)}, f32[1,2,256]{2,1,0:T(2,128)S(1)}, ...), condition=%wide.region_10.11_spmd, body=%wide.region_7.10_spmd.sunk | while | flops 411174400 | bytes 14255189 | solution.py:108
  229.8 1.8 bitcast_reduce_fusion.2
  231.6 2.0 fusion.97
  233.6 0.7 fusion.96
  234.3 1.8 bitcast_reduce_fusion.2
  236.2 2.0 fusion.97
  238.1 0.7 fusion.96
  238.9 1.8 bitcast_reduce_fusion.2
  240.7 2.0 fusion.97
  242.7 0.7 fusion.96
  243.4 1.8 bitcast_reduce_fusion.2
  245.2 2.0 fusion.97
  247.2 0.7 fusion.96
  247.9 1.8 bitcast_reduce_fusion.2
  249.8 2.0 fusion.97
  251.7 0.7 fusion.96
  252.5 1.8 bitcast_reduce_fusion.2
  254.3 2.0 fusion.97
  256.3 0.7 fusion.96
  257.0 1.8 bitcast_reduce_fusion.2
  258.9 2.0 fusion.97
  260.8 0.7 fusion.96
  261.6 1.8 bitcast_reduce_fusion.2
  263.4 2.0 fusion.97
  265.4 0.7 fusion.96
  266.4 0.5 convolution_convert_fusion
  266.9 14.9 %all_to_all.11 = bf16[4,64,2048]{2,1,0:T(8,128)(2,1)S(1)} all-to-all(bf16[4,64,2048]{2,1,0:T(8,128)(2,1)S(1)} %bitcast.172), channel_id=1, replica_groups=mesh['sp_0'=8,'sp_1'=8,'tp'=4,'dp'=2] {'tp'}, dimensions={0} | all-to-all | bytes 2097152 | tf_op jit(solution)/shard_map/all_to_all | solution.py:53
  282.0 0.8 fusion.34
  (60 shorter events, 1.6 us)
Async XLA Ops:
  6.5 259.8 %copy-start = (bf16[128,2048]{1,0:T(8,128)(2,1)S(1)}, bf16[128,2048]{1,0:T(8,128)(2,1)}, u32[]{:S(2)}) copy-start(bf16[128,2048]{1,0:T(8,128)(2,1)} %param.27) | copy-start | bytes 1572868
  6.5 100.3 %copy-start.2 = (bf16[2048,128]{1,0:T(8,128)(2,1)S(1)}, bf16[2048,128]{1,0:T(8,128)(2,1)}, u32[]{:S(2)}) copy-start(bf16[2048,128]{1,0:T(8,128)(2,1)} %param.23) | copy-start | bytes 1572868
  6.5 100.8 %copy-start.3 = (bf16[2048,128]{1,0:T(8,128)(2,1)S(1)}, bf16[2048,128]{1,0:T(8,128)(2,1)}, u32[]{:S(2)}) copy-start(bf16[2048,128]{1,0:T(8,128)(2,1)} %param.22) | copy-start | bytes 1572868
  6.5 204.4 %all-gather.2.cloned.1.call-start = ((), (), s32[]{:S(2)}) async-start(), calls=%async_computation.2 | async-start | bytes 8519680 | tf_op jit(solution)/shard_map/all_gather | solution.py:42
  6.5 102.0 %copy-start.5 = (bf16[1,8,2048]{2,1,0:T(8,128)(2,1)S(1)}, bf16[1,8,2048]{2,1,0:T(8,128)(2,1)}, u32[]{:S(2)}) copy-start(bf16[1,8,2048]{2,1,0:T(8,128)(2,1)} %param.17) | copy-start | bytes 98308
  7.8 100.9 %copy-start.6 = (f32[2048]{0:T(1024)S(1)}, f32[2048]{0:T(1024)}, u32[]{:S(2)}) copy-start(f32[2048]{0:T(1024)} %param.20) | copy-start | bytes 24580
  93.3 65.7 %copy-start.4 = (bf16[2048,128]{1,0:T(8,128)(2,1)S(1)}, bf16[2048,128]{1,0:T(8,128)(2,1)}, u32[]{:S(2)}) copy-start(bf16[2048,128]{1,0:T(8,128)(2,1)} %param.21) | copy-start | bytes 1572868
  93.3 66.2 %copy-start.7 = (f32[1,2]{1,0:T(1,128)S(1)}, f32[1,2]{1,0:T(1,128)}, u32[]{:S(2)}) copy-start(f32[1,2]{1,0:T(1,128)} %param.26) | copy-start | bytes 28
  229.8 36.6 %copy-start.8 = (f32[128]{0:T(128)S(1)}, f32[128]{0:T(128)}, u32[]{:S(2)}) copy-start(f32[128]{0:T(128)} %param.24) | copy-start | bytes 1540
  266.1 15.9 %copy-start.1 = (bf16[1,64,2048]{2,1,0:T(8,128)(2,1)S(1)}, bf16[1,64,2048]{2,1,0:T(8,128)(2,1)}, u32[]{:S(2)}) copy-start(bf16[1,64,2048]{2,1,0:T(8,128)(2,1)} %param.15) | copy-start | bytes 786436
Sparse Core Ops, SparseCore 0:
  108.6 102.3 all-gather.1
where the time goes:
time: 291 us; the launch traced here: 290 us
  blocking collectives  161 us (55%)
  waiting for transfers between devices  50.3 us (17%)
  matrix products  34.6 us (12%)
  local copies, waits for them, and re-layouts  19.1 us (7%)
  between operations  14.3 us (5%)
  other arithmetic  10.4 us (4%)
    psum x3, blocking collectives, by_axis(): shard = lax.psum(shard, axis)  83.1 us
    all_gather x1, waiting for transfers between devices, sent_together(): lax.all_gather(both, axis, axis=dim, tiled=True)  50.3 us
    all_gather x1, blocking collectives, sent_together(): lax.all_gather(both, axis, axis=dim, tiled=True)  49.1 us
    dot_general x9, matrix products, fold_block(): jnp.einsum('hmqk,khe->hmqe', weights.astype(jnp.bfloat16), values_in, pre...  16 us
    dot_general x9, matrix products, fold_block(): jnp.einsum('qhmd,khmd->hmqk', queries, keys_in, preferred_element_type=jn...  14.9 us
    all_to_all x1, blocking collectives, summed_on_arrival(): lax.all_to_all(blocks, axis, split_axis=0, concat_axis=0, tiled=True)  14.9 us
    all_to_all x1, blocking collectives, sent_to_all(): return lax.all_to_all(copies, axis, split_axis=0, concat_axis=0, tiled=True)  13.5 us
    while x2, local copies, waits for them, and re-layouts, fold_keys(): running, ignored = lax.scan(fold_step, running, stacked)  10.6 us
  transfers between devices with their start and end apart: 1, of which 1 were waited for; matrix products, arithmetic and copies ran while one was open for 1% of the time, Pallas kernels for 0%

commit v1 on v0

--- a/solution.py
+++ b/solution.py
@@ -14,7 +14,7 @@
 
 def by_axis(shard, axes):
     for axis in axes:
-        shard = lax.psum(shard, axis)
+        shard = jnp.sum(jax.lax.all_gather(shard, axis), axis=0)
     return shard
 
 

time: 291 us -> 281 us (0.966)
  blocking collectives: 161 us -> 149 us
    psum x3 -> x0, blocking collectives: 83.1 us -> none  [by_axis(): shard = lax.psum(shard, axis)]
    all_gather x0 -> x3, blocking collectives: none -> 70.4 us  [by_axis(): shard = jnp.sum(jax.lax.all_gather(shard, axis), axis=0)]
where the time goes in v1:
time: 281 us; the launch traced here: 280 us
  blocking collectives  149 us (53%)
  waiting for transfers between devices  51.6 us (18%)
  matrix products  34.6 us (12%)
  local copies, waits for them, and re-layouts  19.1 us (7%)
  between operations  14.3 us (5%)
  other arithmetic  10.7 us (4%)
    all_gather x3, blocking collectives, by_axis(): shard = jnp.sum(jax.lax.all_gather(shard, axis), axis=0)  70.4 us
    all_gather x1, waiting for transfers between devices, sent_together(): lax.all_gather(both, axis, axis=dim, tiled=True)  51.6 us
    all_gather x1, blocking collectives, sent_together(): lax.all_gather(both, axis, axis=dim, tiled=True)  49.2 us
    dot_general x9, matrix products, fold_block(): jnp.einsum('hmqk,khe->hmqe', weights.astype(jnp.bfloat16), values_in, pre...  16 us
    dot_general x9, matrix products, fold_block(): jnp.einsum('qhmd,khmd->hmqk', queries, keys_in, preferred_element_type=jn...  14.9 us
    all_to_all x1, blocking collectives, summed_on_arrival(): lax.all_to_all(blocks, axis, split_axis=0, concat_axis=0, tiled=True)  14.9 us
    all_to_all x1, blocking collectives, sent_to_all(): return lax.all_to_all(copies, axis, split_axis=0, concat_axis=0, tiled=True)  14.4 us
    while x2, local copies, waits for them, and re-layouts, fold_keys(): running, ignored = lax.scan(fold_step, running, stacked)  10.6 us
  transfers between devices with their start and end apart: 1, of which 1 were waited for; matrix products, arithmetic and copies ran while one was open for 1% of the time, Pallas kernels for 0%

profile of v1, /device:TPU:8, one launch (start us, length us, event | category | flops | bytes accessed | tf_op | source)
XLA Modules:
  0.0 279.7 jit_solution(8007520951843445950)
XLA Ops:
  6.5 1.2 convolution_bitcast_fusion
  7.8 31.4 %all-gather.3 = f32[8,2,6144]{2,1,0:T(2,128)S(1)} all-gather(f32[1,2,6144]{2,1,0:T(2,128)S(1)} %convolution_bitcast_fusion), channel_id=2, replica_groups=mesh['sp_0'=8,'sp_1'=8,'tp'=4,'dp'=2] {'sp_0'}, dimensions={0}, use_global_device_ids=true | all-gather | bytes 442368 | tf_op jit(solution)/shard_map/all_gather | solution.py:17
  39.3 25.8 %all-gather.4 = f32[8,2,6144]{2,1,0:T(2,128)S(1)} all-gather(f32[1,2,6144]{2,1,0:T(2,128)S(1)} %bitcast.182), channel_id=3, replica_groups=mesh['sp_0'=8,'sp_1'=8,'tp'=4,'dp'=2] {'sp_1'}, dimensions={0}, use_global_device_ids=true | all-gather | bytes 442368 | tf_op jit(solution)/shard_map/all_gather | solution.py:17
  65.2 13.2 %all-gather.5 = f32[4,2,6144]{2,1,0:T(2,128)S(1)} all-gather(f32[1,2,6144]{2,1,0:T(2,128)S(1)} %bitcast.183), channel_id=4, replica_groups=mesh['sp_0'=8,'sp_1'=8,'tp'=4,'dp'=2] {'tp'}, dimensions={0}, use_global_device_ids=true | all-gather | bytes 245760 | tf_op jit(solution)/shard_map/all_gather | solution.py:17
  78.6 1.1 fusion.29
  79.7 1.1 fusion.33
  81.0 14.4 %all_to_all.10 = bf16[4,64,2048]{2,1,0:T(8,128)(2,1)S(1)} all-to-all(bf16[4,64,2048]{2,1,0:T(8,128)(2,1)S(1)} %broadcast_in_dim.13), channel_id=1, replica_groups=mesh['sp_0'=8,'sp_1'=8,'tp'=4,'dp'=2] {'tp'}, dimensions={0} | all-to-all | bytes 2097152 | tf_op jit(solution)/shard_map/all_to_all | solution.py:29
  95.4 0.5 convolution_convert_fusion.1
  95.9 0.5 convolution_convert_fusion.2
  96.4 0.7 pad_maximum_fusion
  97.7 49.2 %all_gather.30 = bf16[512,256]{1,0:T(8,128)(2,1)S(1)} all-gather(bf16[8,256]{1,0:T(8,128)(2,1)S(1)} %pad_maximum_fusion.1), channel_id=1, replica_groups=mesh['sp_0'=8,'sp_1'=8,'tp'=4,'dp'=2] {'sp_0','sp_1'}, dimensions={0}, use_global_device_ids=true | all-gather | bytes 266240 | tf_op jit(solution)/shard_map/all_gather | solution.py:42
  147.8 0.5 convolution_convert_fusion.3
  148.3 0.4 fusion.74
  148.7 0.3 fusion.26
  149.0 0.4 fusion.24
  149.4 51.6 %all-gather.8.cloned.1.call-done = bf16[16384,256]{0,1:T(8,128)(2,1)} async-done(((bf16[256,256]{0,1:T(8,128)(2,1)}), bf16[16384,256]{0,1:T(8,128)(2,1)}) %all-gather.8.cloned.1.call-update) | async-done | bytes 8388624 | tf_op jit(solution)/shard_map/all_gather | solution.py:42
  201.0 5.0 %fusion.71 = (bf16[16384,128]{0,1:T(8,128)(2,1)}, bf16[16384,128]{0,1:T(8,128)(2,1)S(1)}) fusion(bf16[16384,256]{0,1:T(8,128)(2,1)} %all-gather.8.cloned.1.call-done), kind=kLoop, calls=%fused_computation.100 | loop fusion | bytes 16777216 | tf_op jit(solution)/shard_map/split | solution.py:42
  206.1 3.2 %copy.28 = bf16[16,8,8,2048]{3,2,1,0:T(8,128)(2,1)S(1)} copy(bf16[16,8,8,2048]{3,1,2,0:T(8,128)(2,1)S(1)} %bitcast.174) | data formatting | bytes 8388608
  209.3 4.2 %copy.24 = bf16[8,2048,1,2,64]{1,4,3,2,0:T(8,128)(2,1)} copy(bf16[8,2048,1,2,64]{1,0,4,3,2:T(8,128)(2,1)S(1)} %bitcast.170) | data formatting | bytes 8388608 | tf_op jit(solution)/shard_map/while | solution.py:108
  213.5 6.4 %copy.27 = bf16[16384,128]{1,0:T(8,128)(2,1)} copy(bf16[16384,128]{0,1:T(8,128)(2,1)} %get-tuple-element.84) | data formatting | bytes 8388608 | tf_op jit(solution)/shard_map/while | solution.py:108
  219.9 36.3 %while.14 = (s32[]{:T(128)}, f32[1,2,256]{2,1,0:T(2,128)S(1)}, f32[1,2,256]{2,1,0:T(2,128)S(1)}, f32[1,2,256,128]{3,2,1,0:T(8,128)S(1)}, bf16[8,2048,1,2,64]{1,4...) while((s32[]{:T(128)}, f32[1,2,256]{2,1,0:T(2,128)S(1)}, ...), condition=%wide.region_10.11_spmd, body=%wide.region_7.10_spmd.sunk | while | flops 411174400 | bytes 14255189 | solution.py:108
  219.9 1.8 bitcast_reduce_fusion.2
  221.7 2.0 fusion.96
  223.7 0.7 fusion.95
  224.4 1.8 bitcast_reduce_fusion.2
  226.2 2.0 fusion.96
  228.2 0.7 fusion.95
  228.9 1.8 bitcast_reduce_fusion.2
  230.8 2.0 fusion.96
  232.7 0.7 fusion.95
  233.5 1.8 bitcast_reduce_fusion.2
  235.3 2.0 fusion.96
  237.3 0.7 fusion.95
  238.0 1.8 bitcast_reduce_fusion.2
  239.8 2.0 fusion.96
  241.8 0.7 fusion.95
  242.6 1.8 bitcast_reduce_fusion.2
  244.4 2.0 fusion.96
  246.3 0.7 fusion.95
  247.1 1.8 bitcast_reduce_fusion.2
  248.9 2.0 fusion.96
  250.9 0.7 fusion.95
  251.6 1.8 bitcast_reduce_fusion.2
  253.5 2.0 fusion.96
  255.4 0.7 fusion.95
  256.4 0.5 convolution_convert_fusion
  257.0 14.9 %all_to_all.11 = bf16[4,64,2048]{2,1,0:T(8,128)(2,1)S(1)} all-to-all(bf16[4,64,2048]{2,1,0:T(8,128)(2,1)S(1)} %bitcast.176), channel_id=1, replica_groups=mesh['sp_0'=8,'sp_1'=8,'tp'=4,'dp'=2] {'tp'}, dimensions={0} | all-to-all | bytes 2097152 | tf_op jit(solution)/shard_map/all_to_all | solution.py:53
  272.1 0.8 fusion.34
  (63 shorter events, 1.9 us)
Async XLA Ops:
  6.5 249.9 %copy-start = (bf16[128,2048]{1,0:T(8,128)(2,1)S(1)}, bf16[128,2048]{1,0:T(8,128)(2,1)}, u32[]{:S(2)}) copy-start(bf16[128,2048]{1,0:T(8,128)(2,1)} %param.27) | copy-start | bytes 1572868
  6.5 88.9 %copy-start.2 = (bf16[2048,128]{1,0:T(8,128)(2,1)S(1)}, bf16[2048,128]{1,0:T(8,128)(2,1)}, u32[]{:S(2)}) copy-start(bf16[2048,128]{1,0:T(8,128)(2,1)} %param.23) | copy-start | bytes 1572868
  6.5 89.4 %copy-start.3 = (bf16[2048,128]{1,0:T(8,128)(2,1)S(1)}, bf16[2048,128]{1,0:T(8,128)(2,1)}, u32[]{:S(2)}) copy-start(bf16[2048,128]{1,0:T(8,128)(2,1)} %param.22) | copy-start | bytes 1572868
  6.5 194.5 %all-gather.8.cloned.1.call-start = ((), (), s32[]{:S(2)}) async-start(), calls=%async_computation.2 | async-start | bytes 8519680 | tf_op jit(solution)/shard_map/all_gather | solution.py:42
  65.2 31.9 %copy-start.5 = (bf16[1,8,2048]{2,1,0:T(8,128)(2,1)S(1)}, bf16[1,8,2048]{2,1,0:T(8,128)(2,1)}, u32[]{:S(2)}) copy-start(bf16[1,8,2048]{2,1,0:T(8,128)(2,1)} %param.17) | copy-start | bytes 98308
  78.5 18.8 %copy-start.6 = (f32[2048]{0:T(1024)S(1)}, f32[2048]{0:T(1024)}, u32[]{:S(2)}) copy-start(f32[2048]{0:T(1024)} %param.20) | copy-start | bytes 24580
  81.0 66.8 %copy-start.4 = (bf16[2048,128]{1,0:T(8,128)(2,1)S(1)}, bf16[2048,128]{1,0:T(8,128)(2,1)}, u32[]{:S(2)}) copy-start(bf16[2048,128]{1,0:T(8,128)(2,1)} %param.21) | copy-start | bytes 1572868
  81.0 67.3 %copy-start.7 = (f32[1,2]{1,0:T(1,128)S(1)}, f32[1,2]{1,0:T(1,128)}, u32[]{:S(2)}) copy-start(f32[1,2]{1,0:T(1,128)} %param.26) | copy-start | bytes 28
  219.9 36.6 %copy-start.8 = (f32[128]{0:T(128)S(1)}, f32[128]{0:T(128)}, u32[]{:S(2)}) copy-start(f32[128]{0:T(128)} %param.24) | copy-start | bytes 1540
  256.2 15.9 %copy-start.1 = (bf16[1,64,2048]{2,1,0:T(8,128)(2,1)S(1)}, bf16[1,64,2048]{2,1,0:T(8,128)(2,1)}, u32[]{:S(2)}) copy-start(bf16[1,64,2048]{2,1,0:T(8,128)(2,1)} %param.15) | copy-start | bytes 786436
Sparse Core Ops, SparseCore 0:
  97.2 103.7 all-gather.7
